TPU v7x, 32 devices: a whole 2x2x4 slice. The times are simulated.
32 devices in a mesh: dp: 4 (over y, x), kv: 4 (over z), tp: 2 (over core).
Axes of the slice: x: 2, y: 2, z: 4, core: 2. Of those that a mesh axis runs over, the one named last changes fastest.
Arguments:
- tokens: bfloat16 [32, 4096], P('dp', ('kv', 'tp')), may hold values from -7 to 7
- mix_gain: float32 [4096], replicated, may hold values from 0.1 to 1.9
- query_weight: bfloat16 [16, 128, 4096], P('tp', 'kv'), may hold values from -0.09375 to 0.09375
- forget_weight: bfloat16 [16, 128, 4096], P('tp', 'kv'), may hold values from -0.09375 to 0.09375
- value_weight: bfloat16 [16, 128, 4096], P('tp', 'kv'), may hold values from -0.09375 to 0.09375
- gate_weight: bfloat16 [16, 128, 4096], P('tp', 'kv'), may hold values from -0.09375 to 0.09375
- lower_bound: float32 [16, 128], P('tp'), may hold values from 0.02 to 0.9
- recurrent_state: float32 [32, 16, 128, 128], P(('dp', 'kv'), 'tp'), may hold values from -3 to 3
- head_gain: float32 [16, 128], P('tp'), may hold values from 0.1 to 1.9
- out_weight: bfloat16 [16, 128, 4096], P(None, None, ('kv', 'tp')), may hold values from -0.125 to 0.125
- mlp_gain: float32 [4096], replicated, may hold values from 0.1 to 1.9
- up_weight: bfloat16 [4096, 16384], P(None, ('kv', 'tp')), may hold values from -0.09375 to 0.09375
- down_weight: bfloat16 [16384, 4096], P(('kv', 'tp')), may hold values from -0.0625 to 0.0625
Outputs:
- layer_output: bfloat16 [32, 4096], P('dp', ('kv', 'tp'))
- next_state: float32 [32, 16, 128, 128], P(('dp', 'kv'), 'tp')
All inputs are finite; a program needn't handle non-finite values.
Results may differ from a plain program's by a relative error of at most 0.0072.
Values may be sent and summed in bfloat16 or wider, within the bound.
A program may use at most 128 MiB of HBM per device.

v0:
```python
import jax
import jax.numpy as jnp
from jax import lax
from jax.sharding import PartitionSpec as P

epsilon = 1e-06


def normed_rows(row_block, gain_vector):
    whole_rows = lax.all_gather(row_block, ("kv", "tp"), axis=1, tiled=True).astype(jnp.float32)
    inv_root = lax.rsqrt(jnp.mean(whole_rows * whole_rows, axis=1, keepdims=True) + epsilon)
    result_rows = (whole_rows * inv_root * gain_vector).astype(jnp.bfloat16)
    return result_rows


def local(
    tokens,
    mix_gain,
    query_weight,
    forget_weight,
    value_weight,
    gate_weight,
    lower_bound,
    recurrent_state,
    head_gain,
    out_weight,
    mlp_gain,
    up_weight,
    down_weight,
):
    normed = normed_rows(tokens, mix_gain)
    local_heads, local_chan, width = query_weight.shape
    stacked = jnp.stack((query_weight, forget_weight, value_weight, gate_weight), axis=0).reshape(
        -1, width
    )
    product = lax.dot_general(
        normed, stacked, (((1,), (1,)), ((), ())), preferred_element_type=jnp.float32
    ).astype(jnp.bfloat16)
    product = product.reshape(normed.shape[0], 4, local_heads, local_chan)
    pre_query, pre_forget, value_rows, pre_gate = (
        lax.all_to_all(product[:, 0], "kv", split_axis=0, concat_axis=2, tiled=True),
        lax.all_to_all(product[:, 1], "kv", split_axis=0, concat_axis=2, tiled=True),
        lax.all_to_all(product[:, 2], "kv", split_axis=0, concat_axis=2, tiled=True),
        lax.all_to_all(product[:, 3], "kv", split_axis=0, concat_axis=2, tiled=True),
    )
    log_forget = jnp.logaddexp(
        jnp.log(lower_bound),
        jnp.log1p(-lower_bound) + jax.nn.log_sigmoid(pre_forget.astype(jnp.float32)),
    )
    key_rows = -jnp.expm1(log_forget)
    next_state = (
        jnp.exp(log_forget)[:, :, :, None] * recurrent_state
        + key_rows[:, :, :, None] * value_rows.astype(jnp.float32)[:, :, None, :]
    )
    query_act = jax.nn.silu(pre_query.astype(jnp.float32))
    readout = jnp.einsum("bhk,bhkv->bhv", query_act, next_state, precision=lax.Precision.HIGHEST)
    inv_head = lax.rsqrt(jnp.mean(readout * readout, axis=2, keepdims=True) + epsilon)
    mixed_heads = (
        readout * inv_head * head_gain * jax.nn.silu(pre_gate.astype(jnp.float32))
    ).astype(jnp.bfloat16)
    all_heads = lax.all_gather(mixed_heads, "tp", axis=1, tiled=True)
    flat_mixed = all_heads.reshape(all_heads.shape[0], -1)
    out_matrix = out_weight.reshape(-1, out_weight.shape[2])
    projected = jnp.dot(
        lax.all_gather(flat_mixed, "kv", axis=0, tiled=True),
        out_matrix,
        preferred_element_type=jnp.float32,
    )
    residual = lax.optimization_barrier(
        (tokens.astype(jnp.float32) + projected).astype(jnp.bfloat16)
    )
    normed_mlp = normed_rows(residual, mlp_gain)
    hidden = jnp.square(
        jax.nn.relu(jnp.dot(normed_mlp, up_weight, preferred_element_type=jnp.float32))
    ).astype(jnp.bfloat16)
    summed = lax.psum_scatter(
        jnp.dot(hidden, down_weight, preferred_element_type=jnp.float32),
        ("kv", "tp"),
        scatter_dimension=1,
        tiled=True,
    )
    layer_output = (residual.astype(jnp.float32) + summed).astype(jnp.bfloat16)
    return (layer_output, next_state)


def solution(mesh):
    placed = (
        P("dp", ("kv", "tp")),
        P(),
        P("tp", "kv", None),
        P("tp", "kv", None),
        P("tp", "kv", None),
        P("tp", "kv", None),
        P("tp", None),
        P(("dp", "kv"), "tp", None, None),
        P("tp", None),
        P(None, None, ("kv", "tp")),
        P(),
        P(None, ("kv", "tp")),
        P(("kv", "tp"), None),
    )
    return jax.shard_map(
        local,
        mesh=mesh,
        in_specs=placed,
        out_specs=(P("dp", ("kv", "tp")), P(("dp", "kv"), "tp", None, None)),
        check_vma=False,
    )
```

profile of v0, /device:TPU:0, one launch (start us, length us, event | category | flops | bytes accessed | tf_op | source)
XLA Modules:
  0.0 148.9 jit_solution(8380039019351915380)
XLA Ops:
  7.2 0.0 copy-start
  7.2 16.0 %all_gather.12 = bf16[8,4096]{1,0:T(8,128)(2,1)S(1)} all-gather(bf16[8,512]{1,0:T(8,128)(2,1)} %param.13), channel_id=1, replica_groups=mesh['dp'=4,'kv'=4,'tp'=2] {'kv','tp'}, dimensions={1}, use_global_device_ids=true | all-gather | bytes 73728 | tf_op jit(solution)/shard_map/all_gather | solution.py:10
  23.2 0.1 fusion.4
  23.4 4.4 %pad_maximum_fusion = bf16[4,8,32,4096]{3,2,1,0:T(8,128)(2,1)S(1)} fusion(bf16[1,8,32,4096]{3,2,1,0:T(8,128)(2,1)} %bitcast.47, bf16[1,8,32,4096]{3,2,1,0:T(8,128)(2,1)} %bitcast.48, bf16[1,8,32,4096]{3,2,1,0:T(8,128)(2,1)} %bitcast.49, bf16[1,8,32,4096]{3,2,1,0:T(8,128)(2,1)} %bitcast.50), kind=kLoop, calls=%fused_computation | loop fusion | flops 12582912 | bytes 16777216 | tf_op jit(solution)/shard_map/stack | solution.py:33
  27.7 0.0 copy-start.5
  27.8 0.0 copy-start.6
  27.8 0.0 copy-start.2
  27.8 0.0 copy-start.4
  27.8 0.0 copy-done.3
  27.8 2.3 %convolution_convert_fusion = bf16[8,1024]{1,0:T(8,128)(2,1)S(1)} fusion(bf16[1024,4096]{1,0:T(8,128)(2,1)S(1)} %bitcast.46, bf16[8,4096]{1,0:T(8,128)(2,1)S(1)} %all_gather.12, f32[4096]{0:T(1024)S(1)} %copy-done.3, f32[8]{0:T(128)S(1)} %add_rsqrt_fusion.2), kind=kOutput, calls=%fused_computation.4 | convolution fusion | flops 67248128 | bytes 8486944 | tf_op jit(solution)/shard_map/dot_general | solution.py:36
  30.1 0.1 reshape.99
  30.2 0.7 reshape.119
  30.9 4.6 %all-to-all-start.1 = ((bf16[4,2,256]{2,1,0:T(2,128)(2,1)}), bf16[4,2,256]{2,1,0:T(2,128)(2,1)S(1)}, u32[]{:S(2)}, u32[]{:S(2)}) async-start(bf16[4,2,256]{2,1,0:T(2,128)(2,1)} %reshape.119), calls=%async_computation.1 | async-start | bytes 8192 | tf_op jit(solution)/shard_map/all_to_all | solution.py:42
  35.6 0.7 reshape.117
  36.2 0.7 reshape.115
  36.9 0.7 reshape.113
  37.6 3.5 %all-to-all-done.1 = bf16[4,2,256]{2,1,0:T(2,128)(2,1)S(1)} async-done(((bf16[4,2,256]{2,1,0:T(2,128)(2,1)}), bf16[4,2,256]{2,1,0:T(2,128)(2,1)S(1)}, u32[]{:S(2)}, u32[]{:S(2)}) %all-to-all-start.1) | async-done | bytes 4128 | tf_op jit(solution)/shard_map/all_to_all | solution.py:42
  41.1 3.2 %all-to-all-start.2 = ((bf16[4,2,256]{2,1,0:T(2,128)(2,1)}), bf16[4,2,256]{2,1,0:T(2,128)(2,1)S(1)}, u32[]{:S(2)}, u32[]{:S(2)}) async-start(bf16[4,2,256]{2,1,0:T(2,128)(2,1)} %reshape.117), calls=%async_computation.2 | async-start | bytes 8192 | tf_op jit(solution)/shard_map/all_to_all | solution.py:43
  44.3 0.1 reshape.120
  44.4 5.4 %all-to-all-done.2 = bf16[4,2,256]{2,1,0:T(2,128)(2,1)S(1)} async-done(((bf16[4,2,256]{2,1,0:T(2,128)(2,1)}), bf16[4,2,256]{2,1,0:T(2,128)(2,1)S(1)}, u32[]{:S(2)}, u32[]{:S(2)}) %all-to-all-start.2) | async-done | bytes 4128 | tf_op jit(solution)/shard_map/all_to_all | solution.py:43
  49.9 3.2 %all-to-all-start = ((bf16[4,2,256]{2,1,0:T(2,128)(2,1)}), bf16[4,2,256]{2,1,0:T(2,128)(2,1)S(1)}, u32[]{:S(2)}, u32[]{:S(2)}) async-start(bf16[4,2,256]{2,1,0:T(2,128)(2,1)} %reshape.115), calls=%async_computation | async-start | bytes 8192 | tf_op jit(solution)/shard_map/all_to_all | solution.py:41
  53.1 0.1 reshape.118
  53.3 0.1 neg.75
  53.4 0.1 reshape.103
  53.4 5.2 %all-to-all-done = bf16[4,2,256]{2,1,0:T(2,128)(2,1)S(1)} async-done(((bf16[4,2,256]{2,1,0:T(2,128)(2,1)}), bf16[4,2,256]{2,1,0:T(2,128)(2,1)S(1)}, u32[]{:S(2)}, u32[]{:S(2)}) %all-to-all-start) | async-done | bytes 4128 | tf_op jit(solution)/shard_map/all_to_all | solution.py:41
  58.7 3.2 %all-to-all-start.3 = ((bf16[4,2,256]{2,1,0:T(2,128)(2,1)}), bf16[4,2,256]{2,1,0:T(2,128)(2,1)S(1)}, u32[]{:S(2)}, u32[]{:S(2)}) async-start(bf16[4,2,256]{2,1,0:T(2,128)(2,1)} %reshape.113), calls=%async_computation.3 | async-start | bytes 8192 | tf_op jit(solution)/shard_map/all_to_all | solution.py:44
  61.9 0.0 reduce-scatter.2.cloned.1.call-start
  62.0 0.1 reshape.116
  62.1 0.1 reshape.102
  62.2 0.1 fusion.23
  62.3 1.8 %multiply_add_fusion = f32[2,8,128,128]{3,2,1,0:T(8,128)S(1)} fusion(f32[2,8,128,128]{3,2,1,0:T(8,128)} %param.20, f32[2,8,128]{2,1,0:T(8,128)S(1)} %reshape.103, f32[2,8,128]{2,1,0:T(8,128)S(1)} %get-tuple-element.7, f32[2,8,128]{2,1,0:T(8,128)S(1)} %get-tuple-element.6), kind=kLoop, calls=%fused_computation.7 | loop fusion | flops 786432 | bytes 2121728 | tf_op jit(solution)/shard_map/add | solution.py:52
  64.1 0.0 copy-start.1
  64.1 1.0 fusion.25
  65.1 0.1 multiply_reduce_fusion
  65.2 2.3 %all-to-all-done.3 = bf16[4,2,256]{2,1,0:T(2,128)(2,1)S(1)} async-done(((bf16[4,2,256]{2,1,0:T(2,128)(2,1)}), bf16[4,2,256]{2,1,0:T(2,128)(2,1)S(1)}, u32[]{:S(2)}, u32[]{:S(2)}) %all-to-all-start.3) | async-done | bytes 4128 | tf_op jit(solution)/shard_map/all_to_all | solution.py:44
  67.5 0.1 reshape.114
  67.6 0.1 reshape.104
  67.7 0.0 copy-done.6
  67.7 0.1 multiply_convert_fusion
  67.8 1.8 %all_gather.13 = bf16[2,16,128]{2,1,0:T(8,128)(2,1)S(1)} all-gather(bf16[2,8,128]{2,1,0:T(8,128)(2,1)S(1)} %multiply_convert_fusion), channel_id=1, replica_groups=mesh['dp'=4,'kv'=4,'tp'=2] {'tp'}, dimensions={1}, use_global_device_ids=true | all-gather | bytes 12288 | tf_op jit(solution)/shard_map/all_gather | solution.py:61
  69.6 13.1 %all-gather = bf16[4,2,2048]{2,1,0:T(2,128)(2,1)S(1)} all-gather(bf16[1,2,2048]{2,1,0:T(2,128)(2,1)S(1)} %reshape.108), channel_id=1, replica_groups=mesh['dp'=4,'kv'=4,'tp'=2] {'kv'}, dimensions={0}, use_global_device_ids=true | all-gather | bytes 40960 | tf_op jit(solution)/shard_map/all_gather | solution.py:65
  82.8 0.4 fusion.2
  83.2 14.0 %all_gather.15 = bf16[8,4096]{1,0:T(8,128)(2,1)S(1)} all-gather(bf16[8,512]{1,0:T(8,128)(2,1)S(1)} %fusion.2), channel_id=1, replica_groups=mesh['dp'=4,'kv'=4,'tp'=2] {'kv','tp'}, dimensions={1}, use_global_device_ids=true | all-gather | bytes 73728 | tf_op jit(solution)/shard_map/all_gather | solution.py:10
  97.2 0.1 fusion.7
  97.3 13.5 %fusion.3 = f32[8,4096]{1,0:T(8,128)} fusion(bf16[2048,4096]{1,0:T(8,128)(2,1)} %param.25, bf16[4096,2048]{1,0:T(8,128)(2,1)} %param.24, bf16[8,4096]{1,0:T(8,128)(2,1)S(1)} %all_gather.15, f32[4096]{0:T(1024)S(1)} %copy-done.4, f32[8]{0:T(128)S(1)} %add_rsqrt_fusion.1), kind=kOutput, calls=%fused_computation.8 | convolution fusion | flops 268615680 | bytes 33767456 | tf_op jit(solution)/shard_map/dot_general | solution.py:77
  110.9 0.0 reduce-scatter.2.cloned.1.call-update
  110.9 29.9 %reduce-scatter.2.cloned.1.call-done = f32[8,512]{1,0:T(8,128)} async-done(((f32[8,4096]{1,0:T(8,128)}), f32[8,512]{1,0:T(8,128)}) %reduce-scatter.2.cloned.1.call-update) | async-done | bytes 16400 | tf_op jit(solution)/shard_map/reduce_scatter | solution.py:76
  140.7 1.3 add_convert_fusion
  (22 shorter events, 0.2 us)
Async XLA Ops:
  7.2 75.6 %copy-start = (bf16[16,128,512]{2,1,0:T(8,128)(2,1)S(1)}, bf16[16,128,512]{2,1,0:T(8,128)(2,1)}, u32[]{:S(2)}) copy-start(bf16[16,128,512]{2,1,0:T(8,128)(2,1)} %param.22) | copy-start | bytes 6291460
  23.4 4.4 %copy-start.3 = (f32[4096]{0:T(1024)S(1)}, f32[4096]{0:T(1024)}, u32[]{:S(2)}) copy-start(f32[4096]{0:T(1024)} %param.14) | copy-start | bytes 49156
  27.7 7.8 %copy-start.5 = (f32[8,128]{1,0:T(8,128)S(1)}, f32[8,128]{1,0:T(8,128)}, u32[]{:S(2)}) copy-start(f32[8,128]{1,0:T(8,128)} %param.19) | copy-start | bytes 12292
  27.8 39.9 %copy-start.6 = (f32[8,128]{1,0:T(8,128)S(1)}, f32[8,128]{1,0:T(8,128)}, u32[]{:S(2)}) copy-start(f32[8,128]{1,0:T(8,128)} %param.21) | copy-start | bytes 12292
  27.8 55.0 %copy-start.2 = (bf16[8,512]{1,0:T(8,128)(2,1)S(1)}, bf16[8,512]{1,0:T(8,128)(2,1)}, u32[]{:S(2)}) copy-start(bf16[8,512]{1,0:T(8,128)(2,1)} %param.13) | copy-start | bytes 24580
  27.8 69.5 %copy-start.4 = (f32[4096]{0:T(1024)S(1)}, f32[4096]{0:T(1024)}, u32[]{:S(2)}) copy-start(f32[4096]{0:T(1024)} %param.23) | copy-start | bytes 49156
  30.9 10.2 %all-to-all-start.1 = ((bf16[4,2,256]{2,1,0:T(2,128)(2,1)}), bf16[4,2,256]{2,1,0:T(2,128)(2,1)S(1)}, u32[]{:S(2)}, u32[]{:S(2)}) async-start(bf16[4,2,256]{2,1,0:T(2,128)(2,1)} %reshape.119), calls=%async_computation.1 | async-start | bytes 8192 | tf_op jit(solution)/shard_map/all_to_all | solution.py:42
  41.1 8.8 %all-to-all-start.2 = ((bf16[4,2,256]{2,1,0:T(2,128)(2,1)}), bf16[4,2,256]{2,1,0:T(2,128)(2,1)S(1)}, u32[]{:S(2)}, u32[]{:S(2)}) async-start(bf16[4,2,256]{2,1,0:T(2,128)(2,1)} %reshape.117), calls=%async_computation.2 | async-start | bytes 8192 | tf_op jit(solution)/shard_map/all_to_all | solution.py:43
  49.9 8.8 %all-to-all-start = ((bf16[4,2,256]{2,1,0:T(2,128)(2,1)}), bf16[4,2,256]{2,1,0:T(2,128)(2,1)S(1)}, u32[]{:S(2)}, u32[]{:S(2)}) async-start(bf16[4,2,256]{2,1,0:T(2,128)(2,1)} %reshape.115), calls=%async_computation | async-start | bytes 8192 | tf_op jit(solution)/shard_map/all_to_all | solution.py:41
  58.7 8.8 %all-to-all-start.3 = ((bf16[4,2,256]{2,1,0:T(2,128)(2,1)}), bf16[4,2,256]{2,1,0:T(2,128)(2,1)S(1)}, u32[]{:S(2)}, u32[]{:S(2)}) async-start(bf16[4,2,256]{2,1,0:T(2,128)(2,1)} %reshape.113), calls=%async_computation.3 | async-start | bytes 8192 | tf_op jit(solution)/shard_map/all_to_all | solution.py:44
  61.9 78.8 %reduce-scatter.2.cloned.1.call-start = ((), (), s32[]{:S(2)}) async-start(), calls=%async_computation.5 | async-start | bytes 147456 | tf_op jit(solution)/shard_map/reduce_scatter | solution.py:76
  64.1 46.7 %copy-start.1 = (f32[2,8,128,128]{3,2,1,0:T(8,128)}, f32[2,8,128,128]{3,2,1,0:T(8,128)S(1)}, u32[]{:S(2)}) copy-start(f32[2,8,128,128]{3,2,1,0:T(8,128)S(1)} %multiply_add_fusion) | copy-start | bytes 3145732
Sparse Core Ops, SparseCore 0:
  111.0 29.6 reduce-scatter.1
where the time goes:
time: 149 us
  waiting for transfers between devices  46.4 us (31%)
  blocking collectives  45 us (30%)
  matrix products  17.1 us (11%)
  starting transfers between devices  14.4 us (10%)
  between operations  14.2 us (10%)
  other arithmetic  8.09 us (5%)
  local copies, waits for them, and re-layouts  3.68 us (2%)
    all_gather x2, blocking collectives, normed_rows(): lax.all_gather(row_block, ('kv', 'tp'), axis=1, tiled=True)  30 us
    reduce_scatter x1, waiting for transfers between devices, local(): lax.psum_scatter(jnp.dot(hidden, down_weight, preferred_element_type=jnp....  29.9 us
    dot_general x1, matrix products, local(): jnp.dot(hidden, down_weight, preferred_element_type=jnp.float32)  13.5 us
    all_gather x1, blocking collectives, local(): lax.all_gather(flat_mixed, 'kv', axis=0, tiled=True)  13.1 us
    all_to_all x1, waiting for transfers between devices, local(): lax.all_to_all(product[:, 2], 'kv', split_axis=0, concat_axis=2, tiled=True)  5.45 us
    all_to_all x1, waiting for transfers between devices, local(): lax.all_to_all(product[:, 0], 'kv', split_axis=0, concat_axis=2, tiled=True)  5.25 us
    all_to_all x1, starting transfers between devices, local(): lax.all_to_all(product[:, 1], 'kv', split_axis=0, concat_axis=2, tiled=True)  4.64 us
    another operation x1, other arithmetic, local(): jnp.stack((query_weight, forget_weight, value_weight, gate_weight), axis=0)  4.36 us
  transfers between devices with their start and end apart: 5, of which 5 were waited for; matrix products, arithmetic and copies ran while one was open for 4% of the time, Pallas kernels for 0%

commit v1 on v0

--- a/solution.py
+++ b/solution.py
@@ -4,6 +4,18 @@
 from jax.sharding import PartitionSpec as P
 
 epsilon = 1e-06
+
+
+def collect(array, axis, dim):
+    ways, here = (lax.axis_size(axis), lax.axis_index(axis))
+    grown, reach = (array, 1)
+    while reach < ways:
+        theirs = lax.ppermute(grown, axis, [(d, d ^ reach) for d in range(ways)])
+        mine_first = jnp.concatenate([grown, theirs], axis=dim)
+        theirs_first = jnp.concatenate([theirs, grown], axis=dim)
+        grown = jnp.where(here & reach == 0, mine_first, theirs_first)
+        reach = 2 * reach
+    return grown
 
 
 def normed_rows(row_block, gain_vector):
@@ -62,9 +74,7 @@
     flat_mixed = all_heads.reshape(all_heads.shape[0], -1)
     out_matrix = out_weight.reshape(-1, out_weight.shape[2])
     projected = jnp.dot(
-        lax.all_gather(flat_mixed, "kv", axis=0, tiled=True),
-        out_matrix,
-        preferred_element_type=jnp.float32,
+        collect(flat_mixed, "kv", 0), out_matrix, preferred_element_type=jnp.float32
     )
     residual = lax.optimization_barrier(
         (tokens.astype(jnp.float32) + projected).astype(jnp.bfloat16)

time: 149 us -> 145 us (0.973)
  blocking collectives: 45 us -> 31.9 us
  waiting for transfers between devices: 46.4 us -> 53.7 us
    all_gather x1 -> x0, blocking collectives: 13.1 us -> none  [local(): lax.all_gather(flat_mixed, 'kv', axis=0, tiled=True)]
    ppermute x0 -> x2, waiting for transfers between devices: none -> 7.3 us  [collect(): theirs = lax.ppermute(grown, axis, [(d, d ^ reach) for d in range(ways)])]
    unnamed x24 -> x23, local copies, waits for them, and re-layouts: 3.14 us -> 3.11 us
  transfers between devices with their start and end apart: 5 -> 7, of which waited for: 5 -> 7; matrix products, arithmetic and copies ran while one was open for 4% -> 4% of each run, Pallas kernels for 0% -> 0%
where the time goes in v1:
time: 145 us; the launch traced here: 144 us
  waiting for transfers between devices  53.7 us (37%)
  blocking collectives  31.9 us (22%)
  matrix products  17.1 us (12%)
  starting transfers between devices  15.7 us (11%)
  between operations  14.2 us (10%)
  other arithmetic  8.13 us (6%)
  local copies, waits for them, and re-layouts  3.65 us (3%)
    all_gather x2, blocking collectives, normed_rows(): lax.all_gather(row_block, ('kv', 'tp'), axis=1, tiled=True)  30 us
    reduce_scatter x1, waiting for transfers between devices, local(): lax.psum_scatter(jnp.dot(hidden, down_weight, preferred_element_type=jnp....  29.8 us
    dot_general x1, matrix products, local(): jnp.dot(hidden, down_weight, preferred_element_type=jnp.float32)  13.5 us
    ppermute x2, waiting for transfers between devices, collect(): theirs = lax.ppermute(grown, axis, [(d, d ^ reach) for d in range(ways)])  7.3 us
    all_to_all x1, waiting for transfers between devices, local(): lax.all_to_all(product[:, 2], 'kv', split_axis=0, concat_axis=2, tiled=True)  5.45 us
    all_to_all x1, waiting for transfers between devices, local(): lax.all_to_all(product[:, 0], 'kv', split_axis=0, concat_axis=2, tiled=True)  5.25 us
    all_to_all x1, starting transfers between devices, local(): lax.all_to_all(product[:, 1], 'kv', split_axis=0, concat_axis=2, tiled=True)  4.64 us
    another operation x1, other arithmetic, local(): jnp.stack((query_weight, forget_weight, value_weight, gate_weight), axis=0)  4.36 us
  transfers between devices with their start and end apart: 7, of which 7 were waited for; matrix products, arithmetic and copies ran while one was open for 4% of the time, Pallas kernels for 0%

profile of v1, /device:TPU:0, one launch (start us, length us, event | category | flops | bytes accessed | tf_op | source)
XLA Modules:
  0.0 144.3 jit_solution(8344701690101081109)
XLA Ops:
  7.2 0.0 copy-start
  7.2 16.0 %all_gather.9 = bf16[8,4096]{1,0:T(8,128)(2,1)S(1)} all-gather(bf16[8,512]{1,0:T(8,128)(2,1)} %param.13), channel_id=1, replica_groups=mesh['dp'=4,'kv'=4,'tp'=2] {'kv','tp'}, dimensions={1}, use_global_device_ids=true | all-gather | bytes 73728 | tf_op jit(solution)/shard_map/all_gather | solution.py:22
  23.2 0.1 fusion.4
  23.4 4.4 %pad_maximum_fusion = bf16[4,8,32,4096]{3,2,1,0:T(8,128)(2,1)S(1)} fusion(bf16[1,8,32,4096]{3,2,1,0:T(8,128)(2,1)} %bitcast.50, bf16[1,8,32,4096]{3,2,1,0:T(8,128)(2,1)} %bitcast.51, bf16[1,8,32,4096]{3,2,1,0:T(8,128)(2,1)} %bitcast.52, bf16[1,8,32,4096]{3,2,1,0:T(8,128)(2,1)} %bitcast.53), kind=kLoop, calls=%fused_computation | loop fusion | flops 12582912 | bytes 16777216 | tf_op jit(solution)/shard_map/stack | solution.py:45
  27.7 0.0 copy-start.5
  27.8 0.0 copy-start.6
  27.8 0.0 copy-start.2
  27.8 0.0 copy-start.4
  27.8 2.3 %convolution_convert_fusion = bf16[8,1024]{1,0:T(8,128)(2,1)S(1)} fusion(bf16[1024,4096]{1,0:T(8,128)(2,1)S(1)} %bitcast.49, bf16[8,4096]{1,0:T(8,128)(2,1)S(1)} %all_gather.9, f32[4096]{0:T(1024)S(1)} %copy-done.3, f32[8]{0:T(128)S(1)} %add_rsqrt_fusion.2), kind=kOutput, calls=%fused_computation.4 | convolution fusion | flops 67248128 | bytes 8486944 | tf_op jit(solution)/shard_map/dot_general | solution.py:48
  30.1 0.1 reshape.99
  30.2 0.7 reshape.116
  30.9 4.6 %all-to-all-start.1 = ((bf16[4,2,256]{2,1,0:T(2,128)(2,1)}), bf16[4,2,256]{2,1,0:T(2,128)(2,1)S(1)}, u32[]{:S(2)}, u32[]{:S(2)}) async-start(bf16[4,2,256]{2,1,0:T(2,128)(2,1)} %reshape.116), calls=%async_computation.1 | async-start | bytes 8192 | tf_op jit(solution)/shard_map/all_to_all | solution.py:54
  35.5 0.7 reshape.114
  36.2 0.7 reshape.112
  36.9 0.7 reshape.110
  37.6 3.5 %all-to-all-done.1 = bf16[4,2,256]{2,1,0:T(2,128)(2,1)S(1)} async-done(((bf16[4,2,256]{2,1,0:T(2,128)(2,1)}), bf16[4,2,256]{2,1,0:T(2,128)(2,1)S(1)}, u32[]{:S(2)}, u32[]{:S(2)}) %all-to-all-start.1) | async-done | bytes 4128 | tf_op jit(solution)/shard_map/all_to_all | solution.py:54
  41.1 3.2 %all-to-all-start.2 = ((bf16[4,2,256]{2,1,0:T(2,128)(2,1)}), bf16[4,2,256]{2,1,0:T(2,128)(2,1)S(1)}, u32[]{:S(2)}, u32[]{:S(2)}) async-start(bf16[4,2,256]{2,1,0:T(2,128)(2,1)} %reshape.114), calls=%async_computation.2 | async-start | bytes 8192 | tf_op jit(solution)/shard_map/all_to_all | solution.py:55
  44.4 0.1 reshape.117
  44.5 5.4 %all-to-all-done.2 = bf16[4,2,256]{2,1,0:T(2,128)(2,1)S(1)} async-done(((bf16[4,2,256]{2,1,0:T(2,128)(2,1)}), bf16[4,2,256]{2,1,0:T(2,128)(2,1)S(1)}, u32[]{:S(2)}, u32[]{:S(2)}) %all-to-all-start.2) | async-done | bytes 4128 | tf_op jit(solution)/shard_map/all_to_all | solution.py:55
  49.9 3.2 %all-to-all-start = ((bf16[4,2,256]{2,1,0:T(2,128)(2,1)}), bf16[4,2,256]{2,1,0:T(2,128)(2,1)S(1)}, u32[]{:S(2)}, u32[]{:S(2)}) async-start(bf16[4,2,256]{2,1,0:T(2,128)(2,1)} %reshape.112), calls=%async_computation | async-start | bytes 8192 | tf_op jit(solution)/shard_map/all_to_all | solution.py:53
  53.2 0.1 reshape.115
  53.3 0.1 neg.75
  53.4 0.1 reshape.103
  53.5 5.2 %all-to-all-done = bf16[4,2,256]{2,1,0:T(2,128)(2,1)S(1)} async-done(((bf16[4,2,256]{2,1,0:T(2,128)(2,1)}), bf16[4,2,256]{2,1,0:T(2,128)(2,1)S(1)}, u32[]{:S(2)}, u32[]{:S(2)}) %all-to-all-start) | async-done | bytes 4128 | tf_op jit(solution)/shard_map/all_to_all | solution.py:53
  58.7 3.2 %all-to-all-start.3 = ((bf16[4,2,256]{2,1,0:T(2,128)(2,1)}), bf16[4,2,256]{2,1,0:T(2,128)(2,1)S(1)}, u32[]{:S(2)}, u32[]{:S(2)}) async-start(bf16[4,2,256]{2,1,0:T(2,128)(2,1)} %reshape.110), calls=%async_computation.3 | async-start | bytes 8192 | tf_op jit(solution)/shard_map/all_to_all | solution.py:56
  62.0 0.0 reduce-scatter.2.cloned.1.call-start
  62.0 0.1 reshape.113
  62.1 0.1 reshape.102
  62.2 0.1 fusion.30
  62.3 1.8 %multiply_add_fusion = f32[2,8,128,128]{3,2,1,0:T(8,128)S(1)} fusion(f32[2,8,128,128]{3,2,1,0:T(8,128)} %param.20, f32[2,8,128]{2,1,0:T(8,128)S(1)} %reshape.103, f32[2,8,128]{2,1,0:T(8,128)S(1)} %get-tuple-element.7, f32[2,8,128]{2,1,0:T(8,128)S(1)} %get-tuple-element.6), kind=kLoop, calls=%fused_computation.7 | loop fusion | flops 786432 | bytes 2121728 | tf_op jit(solution)/shard_map/add | solution.py:64
  64.1 1.0 fusion.32
  65.1 0.1 multiply_reduce_fusion
  65.2 2.3 %all-to-all-done.3 = bf16[4,2,256]{2,1,0:T(2,128)(2,1)S(1)} async-done(((bf16[4,2,256]{2,1,0:T(2,128)(2,1)}), bf16[4,2,256]{2,1,0:T(2,128)(2,1)S(1)}, u32[]{:S(2)}, u32[]{:S(2)}) %all-to-all-start.3) | async-done | bytes 4128 | tf_op jit(solution)/shard_map/all_to_all | solution.py:56
  67.5 0.1 reshape.111
  67.6 0.1 reshape.104
  67.7 0.1 multiply_convert_fusion
  67.8 1.8 %all_gather.10 = bf16[2,16,128]{2,1,0:T(8,128)(2,1)S(1)} all-gather(bf16[2,8,128]{2,1,0:T(8,128)(2,1)S(1)} %multiply_convert_fusion), channel_id=1, replica_groups=mesh['dp'=4,'kv'=4,'tp'=2] {'tp'}, dimensions={1}, use_global_device_ids=true | all-gather | bytes 12288 | tf_op jit(solution)/shard_map/all_gather | solution.py:73
  69.6 0.7 collective-permute-start
  70.3 3.1 %collective-permute-done = bf16[2,2048]{1,0:T(2,128)(2,1)S(1)} collective-permute-done((bf16[2,2048]{1,0:T(2,128)(2,1)S(1)}, bf16[2,2048]{1,0:T(2,128)(2,1)S(1)}, u32[]{:S(2)}, u32[]{:S(2)}) %collective-permute-start) | collective-permute-done | bytes 8224 | tf_op jit(solution)/shard_map/ppermute | solution.py:13
  73.4 0.6 collective-permute-start.1
  74.0 4.2 %collective-permute-done.1 = bf16[4,2048]{1,0:T(4,128)(2,1)S(1)} collective-permute-done((bf16[4,2048]{1,0:T(4,128)(2,1)S(1)}, bf16[4,2048]{1,0:T(4,128)(2,1)S(1)}, u32[]{:S(2)}, u32[]{:S(2)}) %collective-permute-start.1) | collective-permute-done | bytes 16416 | tf_op jit(solution)/shard_map/ppermute | solution.py:13
  78.3 0.4 fusion.2
  78.6 14.0 %all_gather.11 = bf16[8,4096]{1,0:T(8,128)(2,1)S(1)} all-gather(bf16[8,512]{1,0:T(8,128)(2,1)S(1)} %fusion.2), channel_id=1, replica_groups=mesh['dp'=4,'kv'=4,'tp'=2] {'kv','tp'}, dimensions={1}, use_global_device_ids=true | all-gather | bytes 73728 | tf_op jit(solution)/shard_map/all_gather | solution.py:22
  92.6 0.1 fusion.7
  92.8 13.5 %fusion.3 = f32[8,4096]{1,0:T(8,128)} fusion(bf16[2048,4096]{1,0:T(8,128)(2,1)} %param.25, bf16[4096,2048]{1,0:T(8,128)(2,1)} %param.24, bf16[8,4096]{1,0:T(8,128)(2,1)S(1)} %all_gather.11, f32[4096]{0:T(1024)S(1)} %copy-done.4, f32[8]{0:T(128)S(1)} %add_rsqrt_fusion.1), kind=kOutput, calls=%fused_computation.8 | convolution fusion | flops 268615680 | bytes 33767456 | tf_op jit(solution)/shard_map/dot_general | solution.py:87
  106.3 0.0 reduce-scatter.2.cloned.1.call-update
  106.3 29.8 %reduce-scatter.2.cloned.1.call-done = f32[8,512]{1,0:T(8,128)} async-done(((f32[8,4096]{1,0:T(8,128)}), f32[8,512]{1,0:T(8,128)}) %reduce-scatter.2.cloned.1.call-update) | async-done | bytes 16400 | tf_op jit(solution)/shard_map/reduce_scatter | solution.py:86
  136.2 1.3 add_convert_fusion
  (25 shorter events, 0.2 us)
Async XLA Ops:
  7.2 71.1 %copy-start = (bf16[16,128,512]{2,1,0:T(8,128)(2,1)S(1)}, bf16[16,128,512]{2,1,0:T(8,128)(2,1)}, u32[]{:S(2)}) copy-start(bf16[16,128,512]{2,1,0:T(8,128)(2,1)} %param.22) | copy-start | bytes 6291460
  23.4 4.4 %copy-start.3 = (f32[4096]{0:T(1024)S(1)}, f32[4096]{0:T(1024)}, u32[]{:S(2)}) copy-start(f32[4096]{0:T(1024)} %param.14) | copy-start | bytes 49156
  27.7 7.8 %copy-start.5 = (f32[8,128]{1,0:T(8,128)S(1)}, f32[8,128]{1,0:T(8,128)}, u32[]{:S(2)}) copy-start(f32[8,128]{1,0:T(8,128)} %param.19) | copy-start | bytes 12292
  27.8 40.0 %copy-start.6 = (f32[8,128]{1,0:T(8,128)S(1)}, f32[8,128]{1,0:T(8,128)}, u32[]{:S(2)}) copy-start(f32[8,128]{1,0:T(8,128)} %param.21) | copy-start | bytes 12292
  27.8 50.5 %copy-start.2 = (bf16[8,512]{1,0:T(8,128)(2,1)S(1)}, bf16[8,512]{1,0:T(8,128)(2,1)}, u32[]{:S(2)}) copy-start(bf16[8,512]{1,0:T(8,128)(2,1)} %param.13) | copy-start | bytes 24580
  27.8 65.0 %copy-start.4 = (f32[4096]{0:T(1024)S(1)}, f32[4096]{0:T(1024)}, u32[]{:S(2)}) copy-start(f32[4096]{0:T(1024)} %param.23) | copy-start | bytes 49156
  30.9 10.2 %all-to-all-start.1 = ((bf16[4,2,256]{2,1,0:T(2,128)(2,1)}), bf16[4,2,256]{2,1,0:T(2,128)(2,1)S(1)}, u32[]{:S(2)}, u32[]{:S(2)}) async-start(bf16[4,2,256]{2,1,0:T(2,128)(2,1)} %reshape.116), calls=%async_computation.1 | async-start | bytes 8192 | tf_op jit(solution)/shard_map/all_to_all | solution.py:54
  41.1 8.8 %all-to-all-start.2 = ((bf16[4,2,256]{2,1,0:T(2,128)(2,1)}), bf16[4,2,256]{2,1,0:T(2,128)(2,1)S(1)}, u32[]{:S(2)}, u32[]{:S(2)}) async-start(bf16[4,2,256]{2,1,0:T(2,128)(2,1)} %reshape.114), calls=%async_computation.2 | async-start | bytes 8192 | tf_op jit(solution)/shard_map/all_to_all | solution.py:55
  49.9 8.8 %all-to-all-start = ((bf16[4,2,256]{2,1,0:T(2,128)(2,1)}), bf16[4,2,256]{2,1,0:T(2,128)(2,1)S(1)}, u32[]{:S(2)}, u32[]{:S(2)}) async-start(bf16[4,2,256]{2,1,0:T(2,128)(2,1)} %reshape.112), calls=%async_computation | async-start | bytes 8192 | tf_op jit(solution)/shard_map/all_to_all | solution.py:53
  58.7 8.8 %all-to-all-start.3 = ((bf16[4,2,256]{2,1,0:T(2,128)(2,1)}), bf16[4,2,256]{2,1,0:T(2,128)(2,1)S(1)}, u32[]{:S(2)}, u32[]{:S(2)}) async-start(bf16[4,2,256]{2,1,0:T(2,128)(2,1)} %reshape.110), calls=%async_computation.3 | async-start | bytes 8192 | tf_op jit(solution)/shard_map/all_to_all | solution.py:56
  62.0 74.2 %reduce-scatter.2.cloned.1.call-start = ((), (), s32[]{:S(2)}) async-start(), calls=%async_computation.5 | async-start | bytes 147456 | tf_op jit(solution)/shard_map/reduce_scatter | solution.py:86
  64.1 42.2 %copy-start.1 = (f32[2,8,128,128]{3,2,1,0:T(8,128)}, f32[2,8,128,128]{3,2,1,0:T(8,128)S(1)}, u32[]{:S(2)}) copy-start(f32[2,8,128,128]{3,2,1,0:T(8,128)S(1)} %multiply_add_fusion) | copy-start | bytes 3145732
  69.6 3.7 %collective-permute-start = (bf16[2,2048]{1,0:T(2,128)(2,1)S(1)}, bf16[2,2048]{1,0:T(2,128)(2,1)S(1)}, u32[]{:S(2)}, u32[]{:S(2)}) collective-permute-start(bf16[2,2048]{1,0:T(2,128)(2,1)S(1)} %bitcast.62), channel_id=1, source_target_pairs={{0,2},{2,0},{4,6},{6,4},{1,3},{3,1},{5,7},{7,5},{8,10},{10,8},{12,... | collective-permute-start | bytes 24584 | tf_op jit(solution)/shard_map/ppermute | solution.py:13
  73.4 4.9 %collective-permute-start.1 = (bf16[4,2048]{1,0:T(4,128)(2,1)S(1)}, bf16[4,2048]{1,0:T(4,128)(2,1)S(1)}, u32[]{:S(2)}, u32[]{:S(2)}) collective-permute-start(bf16[4,2048]{1,0:T(4,128)(2,1)S(1)} %maximum_select_fusion.2), channel_id=1, source_target_pairs={{0,4},{2,6},{4,0},{6,2},{1,5},{3,7},{5,1},{7,3},{8,12},{10,14},{12... | collective-permute-start | bytes 49160 | tf_op jit(solution)/shard_map/ppermute | solution.py:13
Sparse Core Ops, SparseCore 0:
  106.5 29.6 reduce-scatter.1
